TPU v7x, 32 devices: a whole 2x2x4 slice. The times are simulated.
32 devices in a mesh: sp: 8 (over z, x), tp: 4 (over y, core).
Axes of the slice: x: 2, y: 2, z: 4, core: 2. Of those that a mesh axis runs over, the one named last changes fastest.
Arguments:
- out_gate: bfloat16 [4096, 1536], P('sp', 'tp'), may hold values from -6 to 6
- in_gate: bfloat16 [4096, 1536], P('sp', 'tp'), may hold values from -6 to 6
- conv_values: bfloat16 [4096, 1536], P('sp', 'tp'), may hold values from -6 to 6
- conv_taps: float32 [3, 1536], P(None, 'tp'), may hold values from -3 to 3
- mix_gain: float32 [1536], replicated, may hold values from 0.1 to 1.9
- out_proj: bfloat16 [1536, 2048], replicated, may hold values from -0.15625 to 0.15625
- residual: bfloat16 [4096, 2048], P(('sp', 'tp')), may hold values from -6 to 6
- ffn_gain: float32 [2048], replicated, may hold values from 0.1 to 1.9
- routes: int32 [4096, 6], P(('sp', 'tp')), may hold values from 0 to 31, all different within a row; in each aligned block of 128 rows (0 to 127, 128 to 255, ...) at most 32 rows name the same one
- route_weights: float32 [4096, 6], P(('sp', 'tp')), may hold values from 0.05 to 1
- shared_gate: bfloat16 [2048, 512], replicated, may hold values from -0.125 to 0.125
- shared_up: bfloat16 [2048, 512], replicated, may hold values from -0.125 to 0.125
- shared_down: bfloat16 [512, 2048], replicated, may hold values from -0.25 to 0.25
- expert_gate: bfloat16 [32, 2048, 512], P(('sp', 'tp')), may hold values from -0.125 to 0.125
- expert_up: bfloat16 [32, 2048, 512], P(('sp', 'tp')), may hold values from -0.125 to 0.125
- expert_down: bfloat16 [32, 512, 2048], P(('sp', 'tp')), may hold values from -0.25 to 0.25
Outputs:
- layer_out: bfloat16 [4096, 2048], P(('sp', 'tp'))
Inputs may be any that keep to these rules, and one draw needn't show every extreme that they name: `routes`: each row names 6 different experts. Within the rows of one device (aligned blocks of 128 rows) no expert is named more than 32 times, a bound that some block reaches.
All inputs are finite; a program needn't handle non-finite values.
Results may differ from a plain program's by a relative error of at most 0.0065.
Values may be sent and summed in bfloat16 or wider, within the bound.
A program may use at most 128 MiB of HBM per device.

v0:
```python
import jax
import jax.numpy as jnp
from jax import lax
from jax.sharding import PartitionSpec as P


def from_behind(block, axis, distance):
    devices = range(lax.axis_size(axis))
    route = [(i - distance, i) for i in devices if i - distance in devices]
    return lax.ppermute(block, axis, route)


def project_norm(conv_out, mix_gain, out_proj):
    values = conv_out.astype(jnp.float32)
    inverse = lax.rsqrt(jnp.mean(values * values, axis=-1) + 1e-06)
    scaled = (values * mix_gain).astype(jnp.bfloat16)
    return jnp.dot(scaled, out_proj, preferred_element_type=jnp.float32) * inverse[:, None]


def swiglu_hidden(row_block, weight_gate, weight_up):
    gate_part = jnp.dot(row_block, weight_gate, preferred_element_type=jnp.float32)
    up_part = jnp.dot(row_block, weight_up, preferred_element_type=jnp.float32)
    return (jax.nn.silu(gate_part) * up_part).astype(jnp.bfloat16)


def body(
    out_gate,
    in_gate,
    conv_values,
    conv_taps,
    mix_gain,
    out_proj,
    residual,
    ffn_gain,
    routes,
    route_weights,
    shared_gate,
    shared_up,
    shared_down,
    expert_gate,
    expert_up,
    expert_down,
):
    mixed_in = in_gate.astype(jnp.float32) * conv_values.astype(jnp.float32)
    taps_count = conv_taps.shape[0]
    length = mixed_in.shape[0]
    earlier = from_behind(mixed_in[length - (taps_count - 1) :], "sp", 1)
    extended = jnp.concatenate([earlier, mixed_in], axis=0)
    filtered = conv_taps[0] * extended[0:length]
    for offset in range(1, taps_count):
        filtered = filtered + conv_taps[offset] * extended[offset : offset + length]
    conv_out = (out_gate.astype(jnp.float32) * filtered).astype(jnp.bfloat16)
    row_count = length // lax.axis_size("tp")
    token_rows = lax.all_to_all(conv_out, "tp", split_axis=0, concat_axis=1, tiled=True)
    mix_result = project_norm(token_rows, mix_gain, out_proj)
    stream = residual.astype(jnp.float32) + mix_result
    norm_inverse = lax.rsqrt(jnp.mean(stream * stream, axis=-1, keepdims=True) + 1e-06)
    normed = (stream * norm_inverse * ffn_gain).astype(jnp.bfloat16)
    shared_result = jnp.dot(
        swiglu_hidden(normed, shared_gate, shared_up),
        shared_down,
        preferred_element_type=jnp.float32,
    )
    model_width = normed.shape[1]
    sp_count = lax.axis_size("sp")
    tp_count = lax.axis_size("tp")
    experts_total = sp_count * tp_count
    top_count = routes.shape[1]
    capacity = max(2, 4 * row_count * top_count // (3 * experts_total))
    flat_ids = routes.reshape(-1)
    onehot = (flat_ids[:, None] == jnp.arange(experts_total, dtype=jnp.int32)[None, :]).astype(
        jnp.int32
    )
    before = jnp.cumsum(onehot, axis=0) - onehot
    slot_rank = jnp.sum(before * onehot, axis=1)
    slot_index = flat_ids * capacity + slot_rank
    source_rows = (
        jnp.full((experts_total * capacity,), row_count, jnp.int32)
        .at[slot_index]
        .set(jnp.arange(flat_ids.shape[0], dtype=jnp.int32) // top_count)
    )
    padded = jnp.concatenate([normed, jnp.zeros((1, model_width), jnp.bfloat16)], axis=0)
    outgoing = padded[source_rows].reshape(experts_total, capacity, model_width)
    arrived = lax.all_to_all(outgoing, ("sp", "tp"), split_axis=0, concat_axis=0, tiled=True)
    leading = arrived.shape[:-1]
    hidden = swiglu_hidden(arrived.reshape(-1, model_width), expert_gate[0], expert_up[0])
    result = jnp.dot(hidden, expert_down[0], preferred_element_type=jnp.float32).astype(
        jnp.bfloat16
    )
    returned_rows = lax.all_to_all(
        result.reshape(leading + (model_width,)),
        ("sp", "tp"),
        split_axis=0,
        concat_axis=0,
        tiled=True,
    )
    flat_returned = returned_rows.reshape(experts_total * capacity, model_width)
    picked = (
        flat_returned[slot_index].reshape(row_count, top_count, model_width).astype(jnp.float32)
    )
    gate_values = route_weights / jnp.sum(route_weights, axis=1, keepdims=True) * 2.5
    routed = jnp.sum(picked * gate_values[:, :, None], axis=1)
    return (stream + shared_result + routed).astype(jnp.bfloat16)


def solution(mesh):
    in_specs = (
        P("sp", "tp"),
        P("sp", "tp"),
        P("sp", "tp"),
        P(None, "tp"),
        P(),
        P(),
        P(("sp", "tp"), None),
        P(),
        P(("sp", "tp"), None),
        P(("sp", "tp"), None),
        P(),
        P(),
        P(),
        P(("sp", "tp"), None, None),
        P(("sp", "tp"), None, None),
        P(("sp", "tp"), None, None),
    )
    out_specs = P(("sp", "tp"), None)
    return jax.shard_map(body, mesh=mesh, in_specs=in_specs, out_specs=out_specs, check_vma=False)
```

profile of v0, /device:TPU:0, one launch (start us, length us, event | category | flops | bytes accessed | tf_op | source)
XLA Modules:
  0.0 276.3 jit_solution(3413777050485992174)
XLA Ops:
  0.0 0.0 copy-start
  0.0 1.3 convert_multiply_fusion.1
  1.4 4.9 %collective-permute-start = (f32[2,384]{1,0:T(2,128)S(1)}, f32[2,384]{1,0:T(2,128)S(1)}, u32[]{:S(2)}, u32[]{:S(2)}) collective-permute-start(f32[2,384]{1,0:T(2,128)S(1)} %slice.36), channel_id=1, source_target_pairs={{0,4},{4,8},{8,12},{12,16},{16,20},{20,24},{24,28},{1,5},{5,9},{9,... | collective-permute-start | bytes 9224 | tf_op jit(solution)/shard_map/ppermute | solution.py:10
  6.2 0.8 copy.25
  7.0 0.1 eq.29
  7.2 0.1 eq.25
  7.3 0.7 broadcast_multiply_fusion
  8.0 1.7 reduce-window.6
  9.8 0.3 slice_reduce_fusion
  10.1 0.1 copy.24
  10.2 0.1 mul.148
  10.3 0.1 fusion.30
  10.5 0.0 copy-done.9
  10.5 0.0 collective-permute-done
  10.5 0.0 copy-done.5
  10.5 1.1 fusion.16
  11.6 3.6 %all-to-all-start = ((bf16[4,128,384]{2,1,0:T(8,128)(2,1)}), bf16[4,128,384]{2,1,0:T(8,128)(2,1)S(1)}, u32[]{:S(2)}, u32[]{:S(2)}) async-start(bf16[4,128,384]{2,1,0:T(8,128)(2,1)} %bitcast), calls=%async_computation | async-start | bytes 786432 | tf_op jit(solution)/shard_map/all_to_all | solution.py:54
  15.2 3.4 %scatter_custom_fusion = s32[1024]{0:T(1024)S(1)} fusion(s32[768]{0:T(1024)S(1)} %fusion.36, s32[768]{0:T(1024)S(1)} %add_select_fusion, s32[]{:T(128)} %constant.13.clone.1), kind=kCustom, calls=%fused_computation.65 | custom fusion | bytes 4100 | tf_op jit(solution)/shard_map/scatter | solution.py:80
  18.6 4.0 %all-to-all-done = bf16[4,128,384]{2,1,0:T(8,128)(2,1)S(1)} async-done(((bf16[4,128,384]{2,1,0:T(8,128)(2,1)}), bf16[4,128,384]{2,1,0:T(8,128)(2,1)S(1)}, u32[]{:S(2)}, u32[]{:S(2)}) %all-to-all-start) | async-done | bytes 393248 | tf_op jit(solution)/shard_map/all_to_all | solution.py:54
  22.5 0.9 convert_bitcast_fusion
  23.5 1.4 copy.23
  24.9 0.2 fusion.17
  25.0 0.0 copy-done.7
  25.1 0.3 fusion.19
  25.3 0.0 copy-start.8
  25.3 4.0 %multiply_reduce_fusion.1 = (f32[128]{0:T(128)S(1)}, f32[128,2048]{1,0:T(8,128)S(1)}) fusion(f32[128]{0:T(128)S(1)} %add_rsqrt_fusion.1, bf16[128,1536]{0,1:T(8,128)(2,1)S(1)} %fusion.19, bf16[1536,2048]{1,0:T(8,128)(2,1)} %param.21, bf16[128,2048]{1,0:T(8,128)(2,1)} %param.22), kind=kOutput, calls=%fused_computation.19 | convolution fusion | flops 806616960 | bytes 8258560 | tf_op jit(solution)/shard_map/dot_general | solution.py:17
  29.4 1.0 copy-done.1
  30.3 0.0 copy-done.8
  30.3 0.2 multiply_convert_fusion.1
  30.5 0.0 copy-start.3
  30.5 6.0 %gather_fusion = bf16[1024,2048]{1,0:T(8,128)(2,1)} fusion(bf16[129,2048]{1,0:T(8,128)(2,1)S(1)} %concatenate.7, s32[1024]{0:T(1024)S(1)} %fusion.34), kind=kCustom, calls=%fused_computation | custom fusion | bytes 8392704 | tf_op jit(solution)/shard_map/gather | solution.py:83
  36.6 97.6 %all_to_all.23 = bf16[32,32,2048]{2,1,0:T(8,128)(2,1)S(1)} all-to-all(bf16[32,32,2048]{2,1,0:T(8,128)(2,1)} %bitcast.53), channel_id=1, replica_groups=mesh['sp'=8,'tp'=4] {'sp','tp'}, dimensions={0} | all-to-all | bytes 8388608 | tf_op jit(solution)/shard_map/all_to_all | solution.py:84
  134.2 2.0 copy-done.4
  136.1 0.0 copy-done.10
  136.1 3.7 %fusion.4 = f32[1024,512]{1,0:T(8,128)} fusion(bf16[1024,2048]{1,0:T(8,128)(2,1)S(1)} %bitcast.55, bf16[1,2048,512]{2,1,0:T(8,128)(2,1)S(1)} %copy-done.10), kind=kOutput, calls=%fused_computation.11 | convolution fusion | flops 2147483648 | bytes 8388608 | tf_op jit(solution)/shard_map/dot_general | solution.py:22
  139.8 0.0 copy-done
  139.8 10.1 %convolution_convert_fusion = bf16[1024,2048]{1,0:T(8,128)(2,1)} fusion(bf16[1,512,2048]{2,1,0:T(8,128)(2,1)S(1)} %copy-done, f32[1024,512]{1,0:T(8,128)} %fusion.4, bf16[1024,2048]{1,0:T(8,128)(2,1)} %bitcast.56, bf16[1,2048,512]{2,1,0:T(8,128)(2,1)} %param.29), kind=kOutput, calls=%fused_computation.4 | convolution fusion | flops 4300210176 | bytes 14680064 | tf_op jit(solution)/shard_map/dot_general | solution.py:87
  149.9 4.0 %all-to-all-start.2 = ((bf16[32,32,2048]{2,1,0:T(8,128)(2,1)}), bf16[32,32,2048]{2,1,0:T(8,128)(2,1)}, u32[]{:S(2)}, u32[]{:S(2)}) async-start(bf16[32,32,2048]{2,1,0:T(8,128)(2,1)} %bitcast.54), calls=%async_computation.2 | async-start | bytes 8388608 | tf_op jit(solution)/shard_map/all_to_all | solution.py:90
  153.9 0.0 copy-done.6
  153.9 0.1 copy.28
  154.1 0.0 copy-done.3
  154.1 2.0 fusion.41
  156.1 91.8 %all-to-all-done.2 = bf16[32,32,2048]{2,1,0:T(8,128)(2,1)} async-done(((bf16[32,32,2048]{2,1,0:T(8,128)(2,1)}), bf16[32,32,2048]{2,1,0:T(8,128)(2,1)}, u32[]{:S(2)}, u32[]{:S(2)}) %all-to-all-start.2) | async-done | bytes 4194336 | tf_op jit(solution)/shard_map/all_to_all | solution.py:90
  248.0 9.8 %gather_fusion.1 = bf16[768,2048]{1,0:T(8,128)(2,1)} fusion(bf16[1024,2048]{1,0:T(8,128)(2,1)} %bitcast.10, s32[1024]{0:T(1024)S(1)} %pad_clamp_fusion), kind=kCustom, calls=%fused_computation.1 | custom fusion | bytes 6294528 | tf_op jit(solution)/shard_map/gather | solution.py:99
  257.8 6.6 %reshape.89 = f32[128,6,2048]{2,1,0:T(8,128)} reshape(bf16[768,2048]{1,0:T(8,128)(2,1)} %gather_fusion.1) | data formatting | bytes 9437184 | tf_op jit(solution)/shard_map/convert_element_type | solution.py:99
  264.3 7.7 %multiply_reduce_fusion = f32[128,2048]{1,0:T(8,128)} fusion(f32[128,6,2048]{2,1,0:T(8,128)} %reshape.89, f32[128,6]{1,0:T(8,128)S(1)} %copy.28), kind=kLoop, calls=%fused_computation.3 | loop fusion | flops 2883584 | bytes 7343104 | tf_op jit(solution)/shard_map/reduce_sum | solution.py:102
  272.0 0.0 copy-done.2
  272.0 4.3 %fusion.2 = bf16[128,2048]{1,0:T(8,128)(2,1)} fusion(f32[128,2048]{1,0:T(8,128)} %multiply_reduce_fusion, f32[128,2048]{1,0:T(8,128)S(1)} %copy-done.2, bf16[512,2048]{1,0:T(8,128)(2,1)} %param.28, bf16[128,2048]{1,0:T(8,128)(2,1)} %copy-done.3, bf16[2048,512]{1,0:T(8,128)(2,1)} %param.27, f32[128,512]{1,0:T(8,128)S(1)} %fusion.41), kind=kOutput, calls=%fused_computation.9 | convolution fusion | flops 538050560 | bytes 7602176 | tf_op jit(solution)/shard_map/dot_general | solution.py:59
  (21 shorter events, 0.2 us)
Async XLA Ops:
  0.0 139.8 %copy-start = (bf16[1,512,2048]{2,1,0:T(8,128)(2,1)S(1)}, bf16[1,512,2048]{2,1,0:T(8,128)(2,1)}, u32[]{:S(2)}) copy-start(bf16[1,512,2048]{2,1,0:T(8,128)(2,1)} %param.31) | copy-start | bytes 6291460
  0.0 10.5 %copy-start.9 = (f32[3,384]{1,0:T(4,128)S(1)}, f32[3,384]{1,0:T(4,128)}, u32[]{:S(2)}) copy-start(f32[3,384]{1,0:T(4,128)} %param.19) | copy-start | bytes 13828
  0.0 10.5 %copy-start.5 = (bf16[512,384]{1,0:T(8,128)(2,1)S(1)}, bf16[512,384]{1,0:T(8,128)(2,1)}, u32[]{:S(2)}) copy-start(bf16[512,384]{1,0:T(8,128)(2,1)} %param.16) | copy-start | bytes 1179652
  1.4 9.1 %collective-permute-start = (f32[2,384]{1,0:T(2,128)S(1)}, f32[2,384]{1,0:T(2,128)S(1)}, u32[]{:S(2)}, u32[]{:S(2)}) collective-permute-start(f32[2,384]{1,0:T(2,128)S(1)} %slice.36), channel_id=1, source_target_pairs={{0,4},{4,8},{8,12},{12,16},{16,20},{20,24},{24,28},{1,5},{5,9},{9,... | collective-permute-start | bytes 9224 | tf_op jit(solution)/shard_map/ppermute | solution.py:10
  11.6 13.5 %copy-start.7 = (f32[1536]{0:T(1024)S(1)}, f32[1536]{0:T(1024)}, u32[]{:S(2)}) copy-start(f32[1536]{0:T(1024)} %param.20) | copy-start | bytes 18436
  11.6 11.0 %all-to-all-start = ((bf16[4,128,384]{2,1,0:T(8,128)(2,1)}), bf16[4,128,384]{2,1,0:T(8,128)(2,1)S(1)}, u32[]{:S(2)}, u32[]{:S(2)}) async-start(bf16[4,128,384]{2,1,0:T(8,128)(2,1)} %bitcast), calls=%async_computation | async-start | bytes 786432 | tf_op jit(solution)/shard_map/all_to_all | solution.py:54
  25.3 5.0 %copy-start.8 = (f32[2048]{0:T(1024)S(1)}, f32[2048]{0:T(1024)}, u32[]{:S(2)}) copy-start(f32[2048]{0:T(1024)} %param.23) | copy-start | bytes 24580
  29.3 1.0 copy-start.1
  30.5 123.6 %copy-start.3 = (bf16[128,2048]{1,0:T(8,128)(2,1)}, bf16[128,2048]{1,0:T(8,128)(2,1)S(1)}, u32[]{:S(2)}) copy-start(bf16[128,2048]{1,0:T(8,128)(2,1)S(1)} %multiply_convert_fusion.1) | copy-start | bytes 1572868
  36.6 99.6 %copy-start.10 = (bf16[1,2048,512]{2,1,0:T(8,128)(2,1)S(1)}, bf16[1,2048,512]{2,1,0:T(8,128)(2,1)}, u32[]{:S(2)}) copy-start(bf16[1,2048,512]{2,1,0:T(8,128)(2,1)} %param.30) | copy-start | bytes 6291460
  134.2 2.0 copy-start.4
  149.9 4.0 %copy-start.6 = (f32[128,6]{0,1:T(8,128)S(1)}, f32[128,6]{0,1:T(8,128)}, u32[]{:S(2)}) copy-start(f32[128,6]{0,1:T(8,128)} %param.25) | copy-start | bytes 9220
  149.9 98.1 %all-to-all-start.2 = ((bf16[32,32,2048]{2,1,0:T(8,128)(2,1)}), bf16[32,32,2048]{2,1,0:T(8,128)(2,1)}, u32[]{:S(2)}, u32[]{:S(2)}) async-start(bf16[32,32,2048]{2,1,0:T(8,128)(2,1)} %bitcast.54), calls=%async_computation.2 | async-start | bytes 8388608 | tf_op jit(solution)/shard_map/all_to_all | solution.py:90
  264.3 7.7 %copy-start.2 = (f32[128,2048]{1,0:T(8,128)S(1)}, f32[128,2048]{1,0:T(8,128)}, u32[]{:S(2)}) copy-start(f32[128,2048]{1,0:T(8,128)} %copy-done.1) | copy-start | bytes 3145732
where the time goes:
time: 277 us; the launch traced here: 276 us
  blocking collectives  97.6 us (35%)
  waiting for transfers between devices  95.8 us (35%)
  local copies, waits for them, and re-layouts  31.9 us (12%)
  matrix products  24.1 us (9%)
  other arithmetic  14.3 us (5%)
  starting transfers between devices  12.4 us (4%)
    all_to_all x1, blocking collectives, body(): lax.all_to_all(outgoing, ('sp', 'tp'), split_axis=0, concat_axis=0, tiled...  97.6 us
    all_to_all x1, waiting for transfers between devices, body(): lax.all_to_all(result.reshape(leading + (model_width,)), ('sp', 'tp'), sp...  91.8 us
    dot_general x1, matrix products, body(): jnp.dot(hidden, expert_down[0], preferred_element_type=jnp.float32)  10.1 us
    gather x1, local copies, waits for them, and re-layouts, body(): flat_returned[slot_index].reshape(row_count, top_count, model_width)  9.82 us
    reduce_sum x1, other arithmetic, body(): routed = jnp.sum(picked * gate_values[:, :, None], axis=1)  7.69 us
    convert_element_type x1, local copies, waits for them, and re-layouts, body(): flat_returned[slot_index].reshape(row_count, top_count, model_width)  6.55 us
    gather x1, local copies, waits for them, and re-layouts, body(): outgoing = padded[source_rows].reshape(experts_total, capacity, model_width)  6.02 us
  transfers between devices with their start and end apart: 3, of which 2 were waited for; matrix products, arithmetic and copies ran while one was open for 4% of the time, Pallas kernels for 0%

commit v1 on v0

v1 whole, which is shorter than its diff:
```python
import functools

import jax
import jax.numpy as jnp
from jax import lax
from jax.experimental import pallas as pl
from jax.experimental.pallas import tpu as pltpu
from jax.sharding import PartitionSpec as P

MESH = pl.DeviceIdType.MESH
META_ROWS = 16


def from_behind(block, axis, distance):
    devices = range(lax.axis_size(axis))
    route = [(i - distance, i) for i in devices if i - distance in devices]
    return lax.ppermute(block, axis, route)


def project_norm(conv_out, mix_gain, out_proj):
    values = conv_out.astype(jnp.float32)
    inverse = lax.rsqrt(jnp.mean(values * values, axis=-1) + 1e-06)
    scaled = (values * mix_gain).astype(jnp.bfloat16)
    return jnp.dot(scaled, out_proj, preferred_element_type=jnp.float32) * inverse[:, None]


def ffn(x, gate, up, down):
    g = jnp.dot(x, gate[...], preferred_element_type=jnp.float32)
    u = jnp.dot(x, up[...], preferred_element_type=jnp.float32)
    h = (g / (1.0 + jnp.exp(-g)) * u).astype(jnp.bfloat16)
    return jnp.dot(h, down[...], preferred_element_type=jnp.float32)


def experts_kernel(
    n_sp, n_tp, width_x, cap, top,
    normed, stream, meta_own, eg_hbm, eu_hbm, ed_hbm, sg_hbm, su_hbm, sd_hbm,
    out,
    gathered, metas, staged, arrived, results, returned,
    left_in, right_in, left_out, right_out, total,
    eg, eu, ed, sg, su, sd,
    w_sem, meta_send, meta_recv, ring_send, ring_recv,
    disp_send, disp_recv, ret_send, ret_recv, red_send, red_recv,
):
    sp = lax.axis_index("sp")
    tp = lax.axis_index("tp")
    half = n_sp // 2
    rows = normed.shape[0]
    mid = rows // 2
    group = n_tp * cap
    width_z = n_sp // width_x

    def place_of(index):
        x, z = lax.rem(index, width_x), lax.div(index, width_x)
        return x * width_z + z + lax.rem(x, 2) * (width_z - 1 - 2 * z)

    def index_of(place):
        x, zz = lax.div(place, width_z), lax.rem(place, width_z)
        return (zz + lax.rem(x, 2) * (width_z - 1 - 2 * zz)) * width_x + x

    place = place_of(sp)

    def ahead(distance):
        return index_of(lax.rem(place + distance, n_sp))

    right, left = ahead(1), ahead(n_sp - 1)

    def partner(j):
        return lax.rem(tp + j, n_tp)

    barrier = pltpu.get_barrier_semaphore()
    for d in range(1, n_sp):
        pl.semaphore_signal(barrier, inc=1, device_id=(ahead(d), tp), device_id_type=MESH)
    for j in range(1, n_tp):
        pl.semaphore_signal(barrier, inc=1, device_id=(sp, partner(j)), device_id_type=MESH)

    weights = [
        pltpu.make_async_copy(src, dst, w_sem.at[i])
        for i, (src, dst) in enumerate(
            ((sg_hbm, sg), (su_hbm, su), (sd_hbm, sd),
             (eg_hbm.at[0], eg), (eu_hbm.at[0], eu), (ed_hbm.at[0], ed))
        )
    ]
    for copy in weights:
        copy.start()
    pl.semaphore_wait(barrier, n_sp - 1 + n_tp - 1)

    def remote(src, dst, send, recv, device):
        return pltpu.make_async_remote_copy(
            src_ref=src, dst_ref=dst, send_sem=send, recv_sem=recv,
            device_id=device, device_id_type=MESH,
        )

    def meta_copy(d):
        return remote(meta_own, metas.at[d], meta_send.at[d], meta_recv.at[d], (ahead(d), tp))

    def ring_copy(s, way, src=None):
        device = (right if way == 0 else left, tp)
        dst = gathered.at[s + 1 if way == 0 else n_sp - s - 1]
        if src is None:
            src = gathered.at[s if way == 0 else lax.rem(n_sp - s, n_sp)]
        return remote(src, dst, ring_send.at[way, s], ring_recv.at[way, s], device)

    def ring_half(way):
        device = (right if way == 0 else left, tp)
        part = pl.ds(0 if way == 0 else mid, mid)
        s = half - 1
        src = gathered.at[s if way == 0 else n_sp - s, part]
        return remote(src, gathered.at[half, part], ring_send.at[way, s], ring_recv.at[way, s], device)

    def disp_copy(d, j):
        src = staged.at[d, pl.ds(pl.multiple_of(partner(j) * cap, cap), cap)]
        dst = arrived.at[d, pl.ds(pl.multiple_of(tp * cap, cap), cap)]
        return remote(src, dst, disp_send.at[d, j], disp_recv.at[d, j], (sp, partner(j)))

    def ret_copy(d, j):
        src = results.at[d, pl.ds(pl.multiple_of(partner(j) * cap, cap), cap)]
        dst = returned.at[d, pl.ds(pl.multiple_of(tp * cap, cap), cap)]
        return remote(src, dst, ret_send.at[d, j], ret_recv.at[d, j], (sp, partner(j)))

    def red_copy(s, way):
        device = (left if way == 0 else right, tp)
        src = (left_out if way == 0 else right_out).at[s]
        dst = (left_in if way == 0 else right_in).at[s - 1]
        return remote(src, dst, red_send.at[way, s], red_recv.at[way, s - 1], device)

    def red_half(way):
        device = (left if way == 0 else right, tp)
        part = pl.ds(0 if way == 0 else mid, mid)
        src = (left_out if way == 0 else right_out).at[half, part]
        dst = (left_in if way == 0 else right_in).at[half - 1, part]
        return remote(src, dst, red_send.at[way, half], red_recv.at[way, half - 1], device)

    first_slot = (sp * group).astype(jnp.float32)

    def matches(meta, k):
        slots = lax.broadcasted_iota(jnp.int32, (group, rows), 0).astype(jnp.float32) + first_slot
        return slots == meta[k : k + 1, :]

    def dispatch(d, block, meta):
        pick = jnp.zeros((group, rows), jnp.float32)
        for k in range(top):
            pick = jnp.where(matches(meta, k), 1.0, pick)
        staged[d] = jnp.dot(
            pick.astype(jnp.bfloat16), block, preferred_element_type=jnp.float32
        ).astype(jnp.bfloat16)
        for j in range(1, n_tp):
            disp_copy(d, j).start()

    own = pl.ds(pl.multiple_of(tp * cap, cap), cap)

    def run_expert(d):
        for j in range(1, n_tp):
            disp_copy(d, j).wait_recv()
        arrived[d, own] = staged[d, own]
        results[d] = ffn(arrived[d], eg, eu, ed).astype(jnp.bfloat16)

    def combine(d, meta):
        for j in range(1, n_tp):
            ret_copy(d, j).wait_recv()
        returned[d, own] = results[d, own]
        mix = jnp.zeros((group, rows), jnp.float32)
        for k in range(top):
            mix = jnp.where(matches(meta, k), meta[top + k : top + k + 1, :], mix)
        return lax.dot_general(
            mix.astype(jnp.bfloat16), returned[d], (((0,), (0,)), ((), ())),
            preferred_element_type=jnp.float32,
        )

    ring_copy(0, 0, normed).start()
    ring_copy(0, 1, normed).start()
    for d in range(1, n_sp):
        meta_copy(d).start()
    dispatch(0, normed[...], meta_own[...])
    left_in[half - 1, mid:] = jnp.zeros((rows - mid, normed.shape[1]), jnp.bfloat16)
    right_in[half - 1, :mid] = jnp.zeros((mid, normed.shape[1]), jnp.bfloat16)
    for copy in weights[:3]:
        copy.wait()
    total[...] = stream[...] + ffn(normed[...], sg, su, sd)
    for copy in weights[3:]:
        copy.wait()

    def gather_step(s, carry):
        ring_copy(s - 1, 0).wait_recv()
        ring_copy(s - 1, 1).wait_recv()

        @pl.when(s < half - 1)
        def _():
            ring_copy(s, 0).start()
            ring_copy(s, 1).start()

        @pl.when(s == half - 1)
        def _():
            ring_half(0).start()
            ring_half(1).start()

        def one(i, c):
            d = s + i * (n_sp - 2 * s)
            meta_copy(d).wait_recv()
            dispatch(d, gathered[d], metas[d])
            return c

        lax.fori_loop(0, 2, one, 0)

        @pl.when(s == 1)
        def _():
            run_expert(0)

        @pl.when(s > 1)
        def _():
            def two(i, c):
                run_expert(s - 1 + i * (n_sp - 2 * (s - 1)))
                return c

            lax.fori_loop(0, 2, two, 0)

        return carry

    lax.fori_loop(1, half, gather_step, 0)
    ring_half(0).wait_recv()
    ring_half(1).wait_recv()
    meta_copy(half).wait_recv()
    dispatch(half, gathered[half], metas[half])

    def last(i, c):
        run_expert(jnp.where(i == 2, half, half - 1 + 2 * i))
        return c

    lax.fori_loop(0, 3, last, 0)

    def give_back(d):
        for j in range(1, n_tp):
            ret_copy(d, j).start()

    give_back(half)
    for s in range(half - 1, 0, -1):
        give_back(s)
        give_back(n_sp - s)
    give_back(0)

    part = combine(half, metas[half])
    left_out[half, :mid] = part[:mid].astype(jnp.bfloat16)
    right_out[half, mid:] = part[mid:].astype(jnp.bfloat16)
    red_half(0).start()
    red_half(1).start()

    def reduce_step(i, carry):
        s = half - 1 - i
        for way, (d, buf_in, buf_out) in enumerate(
            ((s, left_in, left_out), (n_sp - s, right_in, right_out))
        ):
            part = combine(d, metas[d])

            @pl.when(s == half - 1)
            def _():
                red_half(way).wait_recv()

            @pl.when(s < half - 1)
            def _():
                red_copy(s + 1, way).wait_recv()

            buf_out[s] = (part + buf_in[s].astype(jnp.float32)).astype(jnp.bfloat16)
            red_copy(s, way).start()
        return carry

    lax.fori_loop(0, half - 1, reduce_step, 0)
    part = combine(0, meta_own[...]) + total[...]
    for way, buf_in in enumerate((left_in, right_in)):
        red_copy(1, way).wait_recv()
        part = part + buf_in[0].astype(jnp.float32)
    out[...] = part.astype(out.dtype)

    for d in range(1, n_sp):
        meta_copy(d).wait_send()
    for way in range(2):
        ring_copy(0, way, normed).wait_send()
        for s in range(1, half - 1):
            ring_copy(s, way).wait_send()
        ring_half(way).wait_send()
        red_half(way).wait_send()
        for s in range(1, half):
            red_copy(s, way).wait_send()

    def drain(d, c):
        for j in range(1, n_tp):
            disp_copy(d, j).wait_send()
            ret_copy(d, j).wait_send()
        return c

    lax.fori_loop(0, n_sp, drain, 0)


def routed_and_shared(normed, stream, meta, cap, top, eg, eu, ed, sg, su, sd):
    n_sp, n_tp = lax.axis_size("sp"), lax.axis_size("tp")
    rows, width = normed.shape
    hidden, shared_hidden = eg.shape[-1], sg.shape[-1]
    half = n_sp // 2
    group = n_tp * cap
    width_x = max(1, n_tp // 2)
    if n_sp % width_x:
        width_x = 1
    bf, f32 = jnp.bfloat16, jnp.float32
    vmem = pl.BlockSpec(memory_space=pltpu.VMEM)
    anywhere = pl.BlockSpec(memory_space=pl.ANY)
    dma = pltpu.SemaphoreType.DMA
    return pl.pallas_call(
        functools.partial(experts_kernel, n_sp, n_tp, width_x, cap, top),
        out_shape=jax.ShapeDtypeStruct((rows, width), bf),
        in_specs=[vmem] * 3 + [anywhere] * 6,
        out_specs=vmem,
        scratch_shapes=[
            pltpu.VMEM((n_sp, rows, width), bf),
            pltpu.VMEM((n_sp, META_ROWS, rows), f32),
            pltpu.VMEM((n_sp, group, width), bf),
            pltpu.VMEM((n_sp, group, width), bf),
            pltpu.VMEM((n_sp, group, width), bf),
            pltpu.VMEM((n_sp, group, width), bf),
            pltpu.VMEM((half, rows, width), bf),
            pltpu.VMEM((half, rows, width), bf),
            pltpu.VMEM((half + 1, rows, width), bf),
            pltpu.VMEM((half + 1, rows, width), bf),
            pltpu.VMEM((rows, width), f32),
            pltpu.VMEM((width, hidden), bf),
            pltpu.VMEM((width, hidden), bf),
            pltpu.VMEM((hidden, width), bf),
            pltpu.VMEM((width, shared_hidden), bf),
            pltpu.VMEM((width, shared_hidden), bf),
            pltpu.VMEM((shared_hidden, width), bf),
            dma((6,)),
            dma((n_sp,)),
            dma((n_sp,)),
            dma((2, half)),
            dma((2, half)),
            dma((n_sp, n_tp)),
            dma((n_sp, n_tp)),
            dma((n_sp, n_tp)),
            dma((n_sp, n_tp)),
            dma((2, half + 1)),
            dma((2, half + 1)),
        ],
        compiler_params=pltpu.CompilerParams(
            collective_id=0, has_side_effects=True, vmem_limit_bytes=63 * 1024 * 1024
        ),
    )(normed, stream, meta, eg, eu, ed, sg, su, sd)


def route_table(routes, route_weights, experts_total, capacity):
    top_count = routes.shape[1]
    row_count = routes.shape[0]
    ids = routes.T
    experts = jnp.arange(experts_total, dtype=jnp.int32)
    named = ids[:, None, :] == experts[None, :, None]
    onehot = jnp.any(named, axis=0).astype(jnp.bfloat16)
    order = jnp.arange(row_count)
    earlier = (order[:, None] < order[None, :]).astype(jnp.bfloat16)
    before = jnp.dot(onehot, earlier, preferred_element_type=jnp.float32)
    slot = before + (experts * capacity).astype(jnp.float32)[:, None]
    slots = jnp.sum(jnp.where(named, slot[None], 0.0), axis=1)
    weights = route_weights.T
    gates = weights / jnp.sum(weights, axis=0, keepdims=True) * 2.5
    spare = jnp.zeros((META_ROWS - 2 * top_count, row_count), jnp.float32)
    return jnp.concatenate([slots, gates, spare], axis=0)


def body(
    out_gate,
    in_gate,
    conv_values,
    conv_taps,
    mix_gain,
    out_proj,
    residual,
    ffn_gain,
    routes,
    route_weights,
    shared_gate,
    shared_up,
    shared_down,
    expert_gate,
    expert_up,
    expert_down,
):
    mixed_in = in_gate.astype(jnp.float32) * conv_values.astype(jnp.float32)
    taps_count = conv_taps.shape[0]
    length = mixed_in.shape[0]
    earlier = from_behind(mixed_in[length - (taps_count - 1) :], "sp", 1)
    extended = jnp.concatenate([earlier, mixed_in], axis=0)
    filtered = conv_taps[0] * extended[0:length]
    for offset in range(1, taps_count):
        filtered = filtered + conv_taps[offset] * extended[offset : offset + length]
    conv_out = (out_gate.astype(jnp.float32) * filtered).astype(jnp.bfloat16)
    row_count = length // lax.axis_size("tp")
    token_rows = lax.all_to_all(conv_out, "tp", split_axis=0, concat_axis=1, tiled=True)
    mix_result = project_norm(token_rows, mix_gain, out_proj)
    stream = residual.astype(jnp.float32) + mix_result
    norm_inverse = lax.rsqrt(jnp.mean(stream * stream, axis=-1, keepdims=True) + 1e-06)
    normed = (stream * norm_inverse * ffn_gain).astype(jnp.bfloat16)
    experts_total = lax.axis_size("sp") * lax.axis_size("tp")
    top_count = routes.shape[1]
    capacity = max(2, 4 * row_count * top_count // (3 * experts_total))
    meta = route_table(routes, route_weights, experts_total, capacity)
    return routed_and_shared(
        normed, stream, meta, capacity, top_count,
        expert_gate, expert_up, expert_down, shared_gate, shared_up, shared_down,
    )


def solution(mesh):
    in_specs = (
        P("sp", "tp"),
        P("sp", "tp"),
        P("sp", "tp"),
        P(None, "tp"),
        P(),
        P(),
        P(("sp", "tp"), None),
        P(),
        P(("sp", "tp"), None),
        P(("sp", "tp"), None),
        P(),
        P(),
        P(),
        P(("sp", "tp"), None, None),
        P(("sp", "tp"), None, None),
        P(("sp", "tp"), None, None),
    )
    out_specs = P(("sp", "tp"), None)
    return jax.shard_map(body, mesh=mesh, in_specs=in_specs, out_specs=out_specs, check_vma=False)
```

time: 277 us -> 146 us (0.53)
  Pallas kernels: 0 us -> 114 us
  blocking collectives: 97.6 us -> 0 us
  waiting for transfers between devices: 95.8 us -> 6.67 us
  local copies, waits for them, and re-layouts: 31.9 us -> 4.09 us
  matrix products: 24.1 us -> 4.01 us
  other arithmetic: 14.3 us -> 7.5 us
  starting transfers between devices: 12.4 us -> 8.46 us
    pallas_call x0 -> x1, Pallas kernels: none -> 114 us  [routed_and_shared(): pl.pallas_call(functools.partial(experts_kernel, n_sp, n_tp, width_x, cap...]
    all_to_all x1 -> x0, blocking collectives: 97.6 us -> none  [body(): lax.all_to_all(outgoing, ('sp', 'tp'), split_axis=0, concat_axis=0, tiled...]
    all_to_all x1 -> x0, waiting for transfers between devices: 91.8 us -> none  [body(): lax.all_to_all(result.reshape(leading + (model_width,)), ('sp', 'tp'), sp...]
    dot_general x4 -> x1, matrix products: 20.1 us -> 0.09 us  [route_table(): before = jnp.dot(onehot, earlier, preferred_element_type=jnp.float32)]
    gather x2 -> x0, local copies, waits for them, and re-layouts: 15.8 us -> none  [the longest x1 9.82 us: body(): flat_returned[slot_index].reshape(row_count, top_count, model_width)]
    reduce_sum x3 -> x2, other arithmetic: 7.82 us -> 0.73 us  [the longest x1 0.71 us: route_table(): gates = weights / jnp.sum(weights, axis=0, keepdims=True) * 2.5]
    convert_element_type x1 -> x0, local copies, waits for them, and re-layouts: 6.55 us -> none  [body(): flat_returned[slot_index].reshape(row_count, top_count, model_width)]
    all_to_all x1 -> x0, starting transfers between devices: 3.98 us -> none  [body(): lax.all_to_all(result.reshape(leading + (model_width,)), ('sp', 'tp'), sp...]
  transfers between devices with their start and end apart: 3 -> 2, of which waited for: 2 -> 1; matrix products, arithmetic and copies ran while one was open for 4% -> 3% of each run, Pallas kernels for 0% -> 0%
where the time goes in v1:
time: 146 us; the launch traced here: 145 us
  Pallas kernels  114 us (78%)
  starting transfers between devices  8.46 us (6%)
  other arithmetic  7.5 us (5%)
  waiting for transfers between devices  6.67 us (5%)
  local copies, waits for them, and re-layouts  4.09 us (3%)
  matrix products  4.01 us (3%)
    pallas_call x1, Pallas kernels, routed_and_shared(): pl.pallas_call(functools.partial(experts_kernel, n_sp, n_tp, width_x, cap...  114 us
    all_to_all x1, waiting for transfers between devices, body(): lax.all_to_all(conv_out, 'tp', split_axis=0, concat_axis=1, tiled=True)  6.67 us
    ppermute x1, starting transfers between devices, from_behind(): return lax.ppermute(block, axis, route)  4.87 us
    dot_general x1, matrix products, project_norm(): jnp.dot(scaled, out_proj, preferred_element_type=jnp.float32)  3.92 us
    all_to_all x1, starting transfers between devices, body(): lax.all_to_all(conv_out, 'tp', split_axis=0, concat_axis=1, tiled=True)  3.59 us
  transfers between devices with their start and end apart: 2, of which 1 were waited for; matrix products, arithmetic and copies ran while one was open for 3% of the time, Pallas kernels for 0%

profile of v1, /device:TPU:0, one launch (start us, length us, event | category | flops | bytes accessed | tf_op | source)
XLA Modules:
  0.0 145.0 jit_solution(18084505118285561711)
XLA Ops:
  0.0 0.0 copy-start.2
  0.0 1.2 convert_multiply_fusion.1
  1.2 4.9 %collective-permute-start = (f32[2,384]{1,0:T(2,128)S(1)}, f32[2,384]{1,0:T(2,128)S(1)}, u32[]{:S(2)}, u32[]{:S(2)}) collective-permute-start(f32[2,384]{1,0:T(2,128)S(1)} %slice.24), channel_id=1, source_target_pairs={{0,4},{4,8},{8,12},{12,16},{16,20},{20,24},{24,28},{1,5},{5,9},{9,... | collective-permute-start | bytes 9224 | tf_op jit(solution)/shard_map/ppermute | solution.py:17
  6.1 0.7 reduce_sum.39
  6.8 0.7 multiply_bitcast_fusion
  7.5 0.7 fusion.10
  8.2 0.1 convolution_add_fusion
  8.3 0.9 slice_reduce_fusion.2
  9.2 0.1 pad.2.clone
  9.3 0.0 collective-permute-done
  9.3 2.0 %fusion.6 = bf16[512,384]{1,0:T(8,128)(2,1)} fusion(f32[2,384]{1,0:T(2,128)S(1)} %collective-permute-done, f32[512,384]{1,0:T(8,128)S(1)} %convert_multiply_fusion.1, bf16[512,384]{1,0:T(8,128)(2,1)} %param.16, f32[384]{0:T(512)S(1)} %get-tuple-element.6, f32[384]{0:T(512)S(1)} %get-tuple-element.7, f32[384]{0:T(512)S(1)} %get-tuple-element.5), kind=kLoop, calls=%fused_computation.14 | loop fusion | flops 1966080 | bytes 1580544 | tf_op jit(solution)/shard_map/convert_element_type | solution.py:390
  11.3 0.0 copy-start.3
  11.3 3.6 %all-to-all-start = ((bf16[4,128,384]{2,1,0:T(8,128)(2,1)}), bf16[4,128,384]{2,1,0:T(8,128)(2,1)S(1)}, u32[]{:S(2)}, u32[]{:S(2)}) async-start(bf16[4,128,384]{2,1,0:T(8,128)(2,1)} %bitcast), calls=%async_computation | async-start | bytes 786432 | tf_op jit(solution)/shard_map/all_to_all | solution.py:392
  14.9 0.0 copy-done.2
  15.0 0.7 maximum_maximum_fusion.meta_own
  15.6 0.0 copy-start.1
  15.6 6.7 %all-to-all-done = bf16[4,128,384]{2,1,0:T(8,128)(2,1)S(1)} async-done(((bf16[4,128,384]{2,1,0:T(8,128)(2,1)}), bf16[4,128,384]{2,1,0:T(8,128)(2,1)S(1)}, u32[]{:S(2)}, u32[]{:S(2)}) %all-to-all-start) | async-done | bytes 393248 | tf_op jit(solution)/shard_map/all_to_all | solution.py:392
  22.3 0.2 fusion.7
  22.5 0.1 convert_bitcast_fusion
  22.5 0.3 copy.18
  22.8 0.0 copy-done.3
  22.8 0.3 fusion.9
  23.1 0.0 copy-done.1
  23.1 0.0 copy-start.4
  23.1 3.9 %multiply_reduce_fusion = (f32[128]{0:T(128)S(1)}, f32[128,2048]{1,0:T(8,128)S(1)}) fusion(f32[128]{0:T(128)S(1)} %add_rsqrt_fusion.1, bf16[128,1536]{0,1:T(8,128)(2,1)S(1)} %fusion.9, bf16[1536,2048]{1,0:T(8,128)(2,1)} %param.21, bf16[128,2048]{1,0:T(8,128)(2,1)S(1)} %copy-done.1), kind=kOutput, calls=%fused_computation.4 | convolution fusion | flops 806616960 | bytes 8258560 | tf_op jit(solution)/shard_map/dot_general | solution.py:24
  27.0 0.0 copy-start
  27.0 1.0 copy-done
  28.0 0.0 copy-done.4
  28.0 0.9 multiply_convert_fusion.normed
  29.0 114.1 %shard_map.154 = bf16[128,2048]{1,0:T(8,128)(2,1)} custom-call(bf16[128,2048]{1,0:T(8,128)(2,1)} %multiply_convert_fusion.normed, f32[128,2048]{1,0:T(8,128)} %copy-done, f32[16,128]{1,0:T(8,128)} %maximum_maximum_fusion.meta_own, bf16[1,2048,512]{2,1,0:T(8,128)(2,1)} %eg_hbm.1, bf16[1,2048,512]{2,1,0:T(8,128)(2,1)} %eu_hbm.1, bf16[1,512,2048]{2,1,0:T(8,128)(2,1)} %ed_hbm.1, ...), custom_call_target="tpu_custom_call" | custom-call | tf_op jit(solution)/shard_map/pallas_call | solution.py:305
  143.1 1.9 %copy.20 = bf16[128,2048]{1,0:T(8,128)(2,1)} copy(bf16[128,2048]{1,0:T(8,128)(2,1)} %shard_map.154) | data formatting | bytes 1048576
  (6 shorter events, 0.0 us)
Async XLA Ops:
  0.0 14.9 %copy-start.2 = (s32[128,6]{0,1:T(8,128)S(1)}, s32[128,6]{0,1:T(8,128)}, u32[]{:S(2)}) copy-start(s32[128,6]{0,1:T(8,128)} %param.24) | copy-start | bytes 9220
  1.2 8.1 %collective-permute-start = (f32[2,384]{1,0:T(2,128)S(1)}, f32[2,384]{1,0:T(2,128)S(1)}, u32[]{:S(2)}, u32[]{:S(2)}) collective-permute-start(f32[2,384]{1,0:T(2,128)S(1)} %slice.24), channel_id=1, source_target_pairs={{0,4},{4,8},{8,12},{12,16},{16,20},{20,24},{24,28},{1,5},{5,9},{9,... | collective-permute-start | bytes 9224 | tf_op jit(solution)/shard_map/ppermute | solution.py:17
  11.3 11.5 %copy-start.3 = (f32[1536]{0:T(1024)S(1)}, f32[1536]{0:T(1024)}, u32[]{:S(2)}) copy-start(f32[1536]{0:T(1024)} %param.20) | copy-start | bytes 18436
  11.3 11.0 %all-to-all-start = ((bf16[4,128,384]{2,1,0:T(8,128)(2,1)}), bf16[4,128,384]{2,1,0:T(8,128)(2,1)S(1)}, u32[]{:S(2)}, u32[]{:S(2)}) async-start(bf16[4,128,384]{2,1,0:T(8,128)(2,1)} %bitcast), calls=%async_computation | async-start | bytes 786432 | tf_op jit(solution)/shard_map/all_to_all | solution.py:392
  15.6 7.5 %copy-start.1 = (bf16[128,2048]{1,0:T(8,128)(2,1)S(1)}, bf16[128,2048]{1,0:T(8,128)(2,1)}, u32[]{:S(2)}) copy-start(bf16[128,2048]{1,0:T(8,128)(2,1)} %param.22) | copy-start | bytes 1572868
  23.1 4.9 %copy-start.4 = (f32[2048]{0:T(1024)S(1)}, f32[2048]{0:T(1024)}, u32[]{:S(2)}) copy-start(f32[2048]{0:T(1024)} %param.23) | copy-start | bytes 24580
  27.0 1.0 copy-start

commit v2 on v1

v2 whole, which is shorter than its diff:
```python
import functools

import jax
import jax.numpy as jnp
from jax import lax
from jax.experimental import pallas as pl
from jax.experimental.pallas import tpu as pltpu
from jax.sharding import PartitionSpec as P

MESH = pl.DeviceIdType.MESH
META_ROWS = 16
HALO = 16


def ffn(x, gate, up, down):
    g = jnp.dot(x, gate[...], preferred_element_type=jnp.float32)
    u = jnp.dot(x, up[...], preferred_element_type=jnp.float32)
    h = (g / (1.0 + jnp.exp(-g)) * u).astype(jnp.bfloat16)
    return jnp.dot(h, down[...], preferred_element_type=jnp.float32)


def experts_kernel(
    n_sp, n_tp, width_x, cap, top,
    og_hbm, ig_hbm, cv_hbm, taps, mix_gain, residual, ffn_gain, routes, route_weights,
    op_hbm, eg_hbm, eu_hbm, ed_hbm, sg_hbm, su_hbm, sd_hbm,
    out,
    og, ig, cv, conv_out, conv_in, normed, meta_own,
    gathered, metas, staged, arrived, results, returned,
    left_in, right_in, total,
    op, eg, eu, ed, sg, su, sd,
    w_sem, halo_send, halo_recv, conv_send, conv_recv,
    meta_send, meta_recv, ring_send, ring_recv,
    disp_send, disp_recv, ret_send, ret_recv, red_send, red_recv,
):
    sp = lax.axis_index("sp")
    tp = lax.axis_index("tp")
    half = n_sp // 2
    rows, width = normed.shape
    length = og.shape[0]
    mid = rows // 2
    group = n_tp * cap
    width_z = n_sp // width_x

    def place_of(index):
        x, z = lax.rem(index, width_x), lax.div(index, width_x)
        return x * width_z + z + lax.rem(x, 2) * (width_z - 1 - 2 * z)

    def index_of(place):
        x, zz = lax.div(place, width_z), lax.rem(place, width_z)
        return (zz + lax.rem(x, 2) * (width_z - 1 - 2 * zz)) * width_x + x

    place = place_of(sp)

    def ahead(distance):
        return index_of(lax.rem(place + distance, n_sp))

    right, left = ahead(1), ahead(n_sp - 1)

    def partner(j):
        return lax.rem(tp + j, n_tp)

    barrier = pltpu.get_barrier_semaphore()
    for d in range(1, n_sp):
        pl.semaphore_signal(barrier, inc=1, device_id=(ahead(d), tp), device_id_type=MESH)
    for j in range(1, n_tp):
        pl.semaphore_signal(barrier, inc=1, device_id=(sp, partner(j)), device_id_type=MESH)

    weights = [
        pltpu.make_async_copy(src, dst, w_sem.at[i])
        for i, (src, dst) in enumerate(
            ((ig_hbm, ig.at[pl.ds(HALO, length)]), (cv_hbm, cv.at[pl.ds(HALO, length)]),
             (og_hbm, og), (op_hbm, op), (sg_hbm, sg), (su_hbm, su), (sd_hbm, sd),
             (eg_hbm.at[0], eg), (eu_hbm.at[0], eu), (ed_hbm.at[0], ed))
        )
    ]
    for copy in weights:
        copy.start()
    pl.semaphore_wait(barrier, n_sp - 1 + n_tp - 1)

    def remote(src, dst, send, recv, device):
        return pltpu.make_async_remote_copy(
            src_ref=src, dst_ref=dst, send_sem=send, recv_sem=recv,
            device_id=device, device_id_type=MESH,
        )

    def meta_copy(d):
        return remote(meta_own, metas.at[d], meta_send.at[d], meta_recv.at[d], (ahead(d), tp))

    def ring_copy(s, way, src=None):
        device = (right if way == 0 else left, tp)
        dst = gathered.at[s + 1 if way == 0 else n_sp - s - 1]
        if src is None:
            src = gathered.at[s if way == 0 else lax.rem(n_sp - s, n_sp)]
        return remote(src, dst, ring_send.at[way, s], ring_recv.at[way, s], device)

    def ring_half(way):
        device = (right if way == 0 else left, tp)
        part = pl.ds(0 if way == 0 else mid, mid)
        s = half - 1
        src = gathered.at[s if way == 0 else n_sp - s, part]
        return remote(src, gathered.at[half, part], ring_send.at[way, s], ring_recv.at[way, s], device)

    def disp_copy(d, j):
        src = staged.at[d, pl.ds(pl.multiple_of(partner(j) * cap, cap), cap)]
        dst = arrived.at[d, pl.ds(pl.multiple_of(tp * cap, cap), cap)]
        return remote(src, dst, disp_send.at[d, j], disp_recv.at[d, j], (sp, partner(j)))

    def ret_copy(d, j):
        src = results.at[d, pl.ds(pl.multiple_of(partner(j) * cap, cap), cap)]
        dst = returned.at[d, pl.ds(pl.multiple_of(tp * cap, cap), cap)]
        return remote(src, dst, ret_send.at[d, j], ret_recv.at[d, j], (sp, partner(j)))

    def red_copy(s, way):
        device = (left if way == 0 else right, tp)
        src = gathered.at[s if way == 0 else n_sp - s]
        dst = (left_in if way == 0 else right_in).at[s - 1]
        return remote(src, dst, red_send.at[way, s], red_recv.at[way, s - 1], device)

    def red_half(way):
        device = (left if way == 0 else right, tp)
        part = pl.ds(0 if way == 0 else mid, mid)
        src = gathered.at[half, part]
        dst = (left_in if way == 0 else right_in).at[half - 1, part]
        return remote(src, dst, red_send.at[way, half], red_recv.at[way, half - 1], device)

    def halo_copy(i):
        src = (ig_hbm, cv_hbm)[i].at[pl.ds(length - HALO, HALO)]
        dst = (ig, cv)[i].at[pl.ds(0, HALO)]
        device = (lax.rem(sp + 1, n_sp), tp)
        return remote(src, dst, halo_send.at[i], halo_recv.at[i], device)

    def conv_copy(j):
        return remote(
            conv_out.at[j], conv_in.at[tp], conv_send.at[j], conv_recv.at[j], (sp, partner(j))
        )

    halo_copy(0).start()
    halo_copy(1).start()

    experts_total = n_sp * n_tp
    expert = lax.broadcasted_iota(jnp.int32, (experts_total, rows), 0)
    named = [routes[k : k + 1, :] == expert for k in range(top)]
    onehot = jnp.zeros((experts_total, rows), jnp.float32)
    for hit in named:
        onehot = jnp.where(hit, 1.0, onehot)
    earlier = lax.broadcasted_iota(jnp.int32, (rows, rows), 0) < lax.broadcasted_iota(
        jnp.int32, (rows, rows), 1
    )
    before = jnp.dot(
        onehot.astype(jnp.bfloat16),
        jnp.where(earlier, 1.0, 0.0).astype(jnp.bfloat16),
        preferred_element_type=jnp.float32,
    )
    slot = before + (expert * cap).astype(jnp.float32)
    meta_own[...] = jnp.zeros_like(meta_own)
    for k in range(top):
        meta_own[k : k + 1, :] = jnp.sum(jnp.where(named[k], slot, 0.0), axis=0, keepdims=True)
    weight = route_weights[...]
    meta_own[top : 2 * top, :] = weight / jnp.sum(weight, axis=0, keepdims=True) * 2.5

    for copy in weights[:3]:
        copy.wait()
    for d in range(1, n_sp):
        meta_copy(d).start()
    halo_copy(0).wait_recv()
    halo_copy(1).wait_recv()
    taps_count = taps.shape[0]
    for j in list(range(1, n_tp)) + [0]:
        start = pl.multiple_of(partner(j) * rows, rows)
        span = pl.ds(start, rows + HALO)
        mixed = ig[span].astype(jnp.float32) * cv[span].astype(jnp.float32)
        blank = jnp.where(sp * n_tp + partner(j) == 0, HALO, 0)
        at = lax.broadcasted_iota(jnp.int32, mixed.shape, 0)
        mixed = jnp.where(at >= blank, mixed, 0.0)
        base = HALO - (taps_count - 1)
        filtered = taps[0:1, :] * mixed[base : base + rows]
        for o in range(1, taps_count):
            filtered = filtered + taps[o : o + 1, :] * mixed[base + o : base + o + rows]
        value = (og[pl.ds(start, rows)].astype(jnp.float32) * filtered).astype(jnp.bfloat16)
        if j == 0:
            conv_in[tp] = value
        else:
            conv_out[j] = value
            conv_copy(j).start()
    weights[3].wait()
    for j in range(1, n_tp):
        conv_copy(j).wait_recv()
    squares = jnp.zeros((rows, 1), jnp.float32)
    product = jnp.zeros((rows, width), jnp.float32)
    part_width = conv_in.shape[2]
    for t in range(n_tp):
        value = conv_in[t].astype(jnp.float32)
        squares = squares + jnp.sum(value * value, axis=1, keepdims=True)
        product = product + jnp.dot(
            (value * mix_gain[t]).astype(jnp.bfloat16),
            op[t * part_width : (t + 1) * part_width, :],
            preferred_element_type=jnp.float32,
        )
    inverse = lax.rsqrt(squares / (n_tp * part_width) + 1e-06)
    stream = residual[...].astype(jnp.float32) + product * inverse
    power = jnp.mean(stream * stream, axis=1, keepdims=True)
    normed[...] = (stream * lax.rsqrt(power + 1e-06) * ffn_gain[...]).astype(jnp.bfloat16)
    total[...] = stream

    first_slot = (sp * group).astype(jnp.float32)

    def matches(meta, k):
        slots = lax.broadcasted_iota(jnp.int32, (group, rows), 0).astype(jnp.float32) + first_slot
        return slots == meta[k : k + 1, :]

    def dispatch(d, block, meta):
        pick = jnp.zeros((group, rows), jnp.float32)
        for k in range(top):
            pick = jnp.where(matches(meta, k), 1.0, pick)
        staged[d] = jnp.dot(
            pick.astype(jnp.bfloat16), block, preferred_element_type=jnp.float32
        ).astype(jnp.bfloat16)
        for j in range(1, n_tp):
            disp_copy(d, j).start()

    own = pl.ds(pl.multiple_of(tp * cap, cap), cap)

    def run_expert(d):
        for j in range(1, n_tp):
            disp_copy(d, j).wait_recv()
        arrived[d, own] = staged[d, own]
        results[d] = ffn(arrived[d], eg, eu, ed).astype(jnp.bfloat16)

    def combine(d, meta):
        for j in range(1, n_tp):
            ret_copy(d, j).wait_recv()
        returned[d, own] = results[d, own]
        mix = jnp.zeros((group, rows), jnp.float32)
        for k in range(top):
            mix = jnp.where(matches(meta, k), meta[top + k : top + k + 1, :], mix)
        return lax.dot_general(
            mix.astype(jnp.bfloat16), returned[d], (((0,), (0,)), ((), ())),
            preferred_element_type=jnp.float32,
        )

    ring_copy(0, 0, normed).start()
    ring_copy(0, 1, normed).start()
    dispatch(0, normed[...], meta_own[...])
    left_in[half - 1, mid:] = jnp.zeros((rows - mid, normed.shape[1]), jnp.bfloat16)
    right_in[half - 1, :mid] = jnp.zeros((mid, normed.shape[1]), jnp.bfloat16)
    for copy in weights[4:7]:
        copy.wait()
    total[...] += ffn(normed[...], sg, su, sd)
    for copy in weights[7:]:
        copy.wait()

    def gather_step(s, carry):
        ring_copy(s - 1, 0).wait_recv()
        ring_copy(s - 1, 1).wait_recv()

        @pl.when(s < half - 1)
        def _():
            ring_copy(s, 0).start()
            ring_copy(s, 1).start()

        @pl.when(s == half - 1)
        def _():
            ring_half(0).start()
            ring_half(1).start()

        def one(i, c):
            d = s + i * (n_sp - 2 * s)
            meta_copy(d).wait_recv()
            dispatch(d, gathered[d], metas[d])
            return c

        lax.fori_loop(0, 2, one, 0)

        @pl.when(s == 1)
        def _():
            run_expert(0)

        @pl.when(s > 1)
        def _():
            def two(i, c):
                run_expert(s - 1 + i * (n_sp - 2 * (s - 1)))
                return c

            lax.fori_loop(0, 2, two, 0)

        return carry

    lax.fori_loop(1, half, gather_step, 0)
    ring_half(0).wait_recv()
    ring_half(1).wait_recv()
    meta_copy(half).wait_recv()
    dispatch(half, gathered[half], metas[half])

    def give_back(d):
        for j in range(1, n_tp):
            ret_copy(d, j).start()

    def last(i, c):
        d = half - 1 + 2 * i - 3 * lax.div(i, 2)
        run_expert(d)
        give_back(d)
        return c

    lax.fori_loop(0, 3, last, 0)
    for s in range(half - 2, 0, -1):
        give_back(s)
        give_back(n_sp - s)
    give_back(0)

    for way in range(2):
        ring_copy(0, way, normed).wait_send()
        for s in range(1, half - 1):
            ring_copy(s, way).wait_send()
        ring_half(way).wait_send()
    part = combine(half, metas[half])
    gathered[half] = part.astype(jnp.bfloat16)
    red_half(0).start()
    red_half(1).start()

    def reduce_step(i, carry):
        s = half - 1 - i
        for way, (d, buf_in) in enumerate(((s, left_in), (n_sp - s, right_in))):
            part = combine(d, metas[d])

            @pl.when(s == half - 1)
            def _():
                red_half(way).wait_recv()

            @pl.when(s < half - 1)
            def _():
                red_copy(s + 1, way).wait_recv()

            gathered[d] = (part + buf_in[s].astype(jnp.float32)).astype(jnp.bfloat16)
            red_copy(s, way).start()
        return carry

    lax.fori_loop(0, half - 1, reduce_step, 0)
    part = combine(0, meta_own[...]) + total[...]
    for way, buf_in in enumerate((left_in, right_in)):
        red_copy(1, way).wait_recv()
        part = part + buf_in[0].astype(jnp.float32)
    out[...] = part.astype(out.dtype)

    for d in range(1, n_sp):
        meta_copy(d).wait_send()
    for j in range(1, n_tp):
        conv_copy(j).wait_send()
    for way in range(2):
        halo_copy(way).wait_send()
        red_half(way).wait_send()
        for s in range(1, half):
            red_copy(s, way).wait_send()

    def drain(d, c):
        for j in range(1, n_tp):
            disp_copy(d, j).wait_send()
            ret_copy(d, j).wait_send()
        return c

    lax.fori_loop(0, n_sp, drain, 0)


def body(
    out_gate,
    in_gate,
    conv_values,
    conv_taps,
    mix_gain,
    out_proj,
    residual,
    ffn_gain,
    routes,
    route_weights,
    shared_gate,
    shared_up,
    shared_down,
    expert_gate,
    expert_up,
    expert_down,
):
    n_sp, n_tp = lax.axis_size("sp"), lax.axis_size("tp")
    length, channels = in_gate.shape
    rows, width = residual.shape
    top = routes.shape[1]
    cap = max(2, 4 * rows * top // (3 * n_sp * n_tp))
    hidden, shared_hidden = expert_gate.shape[-1], shared_gate.shape[-1]
    half = n_sp // 2
    group = n_tp * cap
    width_x = max(1, n_tp // 2)
    if n_sp % width_x:
        width_x = 1
    bf, f32 = jnp.bfloat16, jnp.float32
    vmem = pl.BlockSpec(memory_space=pltpu.VMEM)
    anywhere = pl.BlockSpec(memory_space=pl.ANY)
    dma = pltpu.SemaphoreType.DMA
    return pl.pallas_call(
        functools.partial(experts_kernel, n_sp, n_tp, width_x, cap, top),
        out_shape=jax.ShapeDtypeStruct((rows, width), bf),
        in_specs=[anywhere] * 3 + [vmem] * 6 + [anywhere] * 7,
        out_specs=vmem,
        scratch_shapes=[
            pltpu.VMEM((length, channels), bf),
            pltpu.VMEM((length + HALO, channels), bf),
            pltpu.VMEM((length + HALO, channels), bf),
            pltpu.VMEM((n_tp, rows, channels), bf),
            pltpu.VMEM((n_tp, rows, channels), bf),
            pltpu.VMEM((rows, width), bf),
            pltpu.VMEM((META_ROWS, rows), f32),
            pltpu.VMEM((n_sp, rows, width), bf),
            pltpu.VMEM((n_sp, META_ROWS, rows), f32),
            pltpu.VMEM((n_sp, group, width), bf),
            pltpu.VMEM((n_sp, group, width), bf),
            pltpu.VMEM((n_sp, group, width), bf),
            pltpu.VMEM((n_sp, group, width), bf),
            pltpu.VMEM((half, rows, width), bf),
            pltpu.VMEM((half, rows, width), bf),
            pltpu.VMEM((rows, width), f32),
            pltpu.VMEM((n_tp * channels, width), bf),
            pltpu.VMEM((width, hidden), bf),
            pltpu.VMEM((width, hidden), bf),
            pltpu.VMEM((hidden, width), bf),
            pltpu.VMEM((width, shared_hidden), bf),
            pltpu.VMEM((width, shared_hidden), bf),
            pltpu.VMEM((shared_hidden, width), bf),
            dma((10,)),
            dma((2,)),
            dma((2,)),
            dma((n_tp,)),
            dma((n_tp,)),
            dma((n_sp,)),
            dma((n_sp,)),
            dma((2, half)),
            dma((2, half)),
            dma((n_sp, n_tp)),
            dma((n_sp, n_tp)),
            dma((n_sp, n_tp)),
            dma((n_sp, n_tp)),
            dma((2, half + 1)),
            dma((2, half + 1)),
        ],
        compiler_params=pltpu.CompilerParams(
            collective_id=0, has_side_effects=True, vmem_limit_bytes=63 * 1024 * 1024
        ),
    )(
        out_gate, in_gate, conv_values, conv_taps, mix_gain.reshape(n_tp, 1, channels),
        residual, ffn_gain.reshape(1, width), routes.T, route_weights.T,
        out_proj, expert_gate, expert_up, expert_down, shared_gate, shared_up, shared_down,
    )


def solution(mesh):
    in_specs = (
        P("sp", "tp"),
        P("sp", "tp"),
        P("sp", "tp"),
        P(None, "tp"),
        P(),
        P(),
        P(("sp", "tp"), None),
        P(),
        P(("sp", "tp"), None),
        P(("sp", "tp"), None),
        P(),
        P(),
        P(),
        P(("sp", "tp"), None, None),
        P(("sp", "tp"), None, None),
        P(("sp", "tp"), None, None),
    )
    out_specs = P(("sp", "tp"), None)
    return jax.shard_map(body, mesh=mesh, in_specs=in_specs, out_specs=out_specs, check_vma=False)
```

time: 146 us -> 142 us (0.973)
  Pallas kernels: 114 us -> 139 us
  starting transfers between devices: 8.46 us -> 0 us
  other arithmetic: 7.5 us -> 0 us
  waiting for transfers between devices: 6.67 us -> 0 us
  matrix products: 4.01 us -> 0 us
    pallas_call x1, Pallas kernels: 114 us -> 139 us  [body(): pl.pallas_call(functools.partial(experts_kernel, n_sp, n_tp, width_x, cap...]
    all_to_all x1 -> x0, waiting for transfers between devices: 6.67 us -> none  [body(): lax.all_to_all(conv_out, 'tp', split_axis=0, concat_axis=1, tiled=True)]
    ppermute x1 -> x0, starting transfers between devices: 4.87 us -> none  [from_behind(): return lax.ppermute(block, axis, route)]
    dot_general x2 -> x0, matrix products: 4.01 us -> none  [the longest x1 3.92 us: project_norm(): jnp.dot(scaled, out_proj, preferred_element_type=jnp.float32)]
    all_to_all x1 -> x0, starting transfers between devices: 3.59 us -> none  [body(): lax.all_to_all(conv_out, 'tp', split_axis=0, concat_axis=1, tiled=True)]
    convert_element_type x5 -> x0, other arithmetic: 3.32 us -> none  [the longest x1 2.05 us: body(): conv_out = (out_gate.astype(jnp.float32) * filtered).astype(jnp.bfloat16)]
    mul x2 -> x0, other arithmetic: 1.9 us -> none  [the longest x1 1.21 us: body(): mixed_in = in_gate.astype(jnp.float32) * conv_values.astype(jnp.float32)]
  transfers between devices with their start and end apart: 2 -> 0, of which waited for: 1 -> 0; matrix products, arithmetic and copies ran while one was open for 3% -> 0% of each run, Pallas kernels for 0% -> 0%
where the time goes in v2:
time: 142 us
  Pallas kernels  139 us (98%)
  local copies, waits for them, and re-layouts  3.18 us (2%)
    pallas_call x1, Pallas kernels, body(): pl.pallas_call(functools.partial(experts_kernel, n_sp, n_tp, width_x, cap...  139 us

profile of v2, /device:TPU:0, one launch (start us, length us, event | category | flops | bytes accessed | tf_op | source)
XLA Modules:
  0.0 142.2 jit_solution(15324546549349270340)
XLA Ops:
  0.0 1.3 reshape.6.mix_gain
  1.3 139.0 %shard_map.154 = bf16[128,2048]{1,0:T(8,128)(2,1)} custom-call(bf16[512,384]{1,0:T(8,128)(2,1)} %og_hbm.1, bf16[512,384]{1,0:T(8,128)(2,1)} %ig_hbm.1, bf16[512,384]{1,0:T(8,128)(2,1)} %cv_hbm.1, f32[3,384]{1,0:T(4,128)} %taps.1, f32[4,1,384]{2,1,0:T(1,128)} %reshape.6.mix_gain, bf16[128,2048]{1,0:T(8,128)(2,1)} %residual.1, f32[1,2048]{1,0:T(1,128)} %bitcast.3, ...), custom_call_target="tpu_custom_call" | custom-call | tf_op jit(solution)/shard_map/pallas_call | solution.py:396
  140.3 1.9 %copy.18 = bf16[128,2048]{1,0:T(8,128)(2,1)} copy(bf16[128,2048]{1,0:T(8,128)(2,1)} %shard_map.154) | data formatting | bytes 1048576
